TPU v7x, 32 devices: a whole 2x2x4 slice. The times are simulated.
32 devices in a mesh: rep: 2 (over x), fs: 8 (over z, y), tp: 2 (over core).
Axes of the slice: x: 2, y: 2, z: 4, core: 2. Of those that a mesh axis runs over, the one named last changes fastest.
Arguments:
- inputs: bfloat16 [2048, 2048], P(('rep', 'fs'), 'tp'), may hold values from -6 to 6
- cotangent: bfloat16 [2048, 2048], P(('rep', 'fs'), 'tp'), may hold values from -8 to 8
- gate_weight: bfloat16 [2048, 2816], P('fs', 'tp'), may hold values from -0.125 to 0.125
- up_weight: bfloat16 [2048, 2816], P('fs', 'tp'), may hold values from -0.125 to 0.125
- down_weight: bfloat16 [2816, 2048], P('tp', 'fs'), may hold values from -0.109375 to 0.109375
Outputs:
- grad_inputs: bfloat16 [2048, 2048], P(('rep', 'fs'), 'tp')
- grad_gate_weight: float32 [2048, 2816], P('fs', 'tp')
- grad_up_weight: float32 [2048, 2816], P('fs', 'tp')
- grad_down_weight: float32 [2816, 2048], P('tp', 'fs')
All inputs are finite; a program needn't handle non-finite values.
Results may differ from a plain program's by a relative error of at most 0.014.
Values may be sent and summed in bfloat16 or wider, within the bound.
A program may use at most 64 MiB of HBM per device.

v0:
```python
import jax
import jax.numpy as jnp
from jax import lax
from jax.sharding import PartitionSpec as P


def per_device(inputs, cotangent, gate_weight, up_weight, down_weight):
    input_full, cotan_full = (
        lax.all_gather(inputs, "tp", axis=1, tiled=True),
        lax.all_gather(cotangent, "tp", axis=1, tiled=True),
    )
    contract_last = (((1,), (1,)), ((), ()))
    contract_first = (((0,), (0,)), ((), ()))
    gate_full, up_full = (
        lax.all_gather(gate_weight, "fs", axis=0, tiled=True),
        lax.all_gather(up_weight, "fs", axis=0, tiled=True),
    )
    gate_pre = jnp.dot(input_full, gate_full, preferred_element_type=jnp.float32)
    up_pre = jnp.dot(input_full, up_full, preferred_element_type=jnp.float32)
    grad_hidden = lax.dot_general(
        cotan_full,
        lax.all_gather(down_weight, "fs", axis=1, tiled=True),
        contract_last,
        preferred_element_type=jnp.float32,
    )
    sigmoid_gate = jax.nn.sigmoid(gate_pre)
    activated = gate_pre * sigmoid_gate
    hidden = (activated * up_pre).astype(jnp.bfloat16)
    grad_gate = (
        grad_hidden * up_pre * sigmoid_gate * (1.0 + gate_pre * (1.0 - sigmoid_gate))
    ).astype(jnp.bfloat16)
    grad_up = (grad_hidden * activated).astype(jnp.bfloat16)
    partial_sum = lax.dot_general(
        grad_gate, gate_full, contract_last, preferred_element_type=jnp.float32
    )
    partial_sum = partial_sum + lax.dot_general(
        grad_up, up_full, contract_last, preferred_element_type=jnp.float32
    )
    grad_inputs = lax.psum_scatter(
        partial_sum.astype(jnp.bfloat16), "tp", scatter_dimension=1, tiled=True
    )
    input_blocks, cotan_blocks = (
        lax.all_to_all(input_full, "fs", split_axis=1, concat_axis=0, tiled=True),
        lax.all_to_all(cotan_full, "fs", split_axis=1, concat_axis=0, tiled=True),
    )
    gate_grads = lax.dot_general(
        input_blocks,
        lax.all_gather(grad_gate, "fs", axis=0, tiled=True),
        contract_first,
        preferred_element_type=jnp.float32,
    )
    up_grads = lax.dot_general(
        input_blocks,
        lax.all_gather(grad_up, "fs", axis=0, tiled=True),
        contract_first,
        preferred_element_type=jnp.float32,
    )
    down_grads = lax.dot_general(
        lax.all_gather(hidden, "fs", axis=0, tiled=True),
        cotan_blocks,
        contract_first,
        preferred_element_type=jnp.float32,
    )
    gate_grads, up_grads, down_grads = lax.psum((gate_grads, up_grads, down_grads), "rep")
    return (grad_inputs, gate_grads, up_grads, down_grads)


def solution(mesh):
    placed = (
        P(("rep", "fs"), "tp"),
        P(("rep", "fs"), "tp"),
        P("fs", "tp"),
        P("fs", "tp"),
        P("tp", "fs"),
    )
    return jax.shard_map(
        per_device,
        mesh=mesh,
        in_specs=placed,
        out_specs=(P(("rep", "fs"), "tp"), P("fs", "tp"), P("fs", "tp"), P("tp", "fs")),
        check_vma=False,
    )
```

profile of v0, /device:TPU:0, one launch (start us, length us, event | category | flops | bytes accessed | tf_op | source)
XLA Modules:
  0.0 614.6 jit_solution(6929652493873831406)
XLA Ops:
  7.2 0.0 all-gather.11.cloned.1.call-start
  7.2 0.7 all-gather.11.cloned.1.call-update
  7.9 0.0 all-gather.7.cloned.1.call-start
  7.9 0.7 all-gather.7.cloned.1.call-update
  8.6 0.0 all-gather.9.cloned.1.call-start
  8.7 0.7 all-gather.9.cloned.1.call-update
  9.4 0.0 all-gather.13.cloned.1.call-start
  9.4 1.1 copy.14
  10.6 1.1 copy.13
  11.7 2.3 all_gather.26
  14.0 2.3 all_gather.24
  16.3 88.9 %all-gather.11.cloned.1.call-done = bf16[2048,1408]{1,0:T(8,128)(2,1)} async-done(((bf16[256,1408]{1,0:T(8,128)(2,1)}), bf16[2048,1408]{1,0:T(8,128)(2,1)}) %all-gather.11.cloned.1.call-update) | async-done | bytes 5767184 | tf_op jit(solution)/shard_map/all_gather | solution.py:15
  105.2 3.6 fusion.3
  108.9 89.7 %all-gather.7.cloned.1.call-done = bf16[1408,2048]{1,0:T(8,128)(2,1)} async-done(((bf16[1408,256]{1,0:T(8,128)(2,1)}), bf16[1408,2048]{1,0:T(8,128)(2,1)}) %all-gather.7.cloned.1.call-update) | async-done | bytes 5767184 | tf_op jit(solution)/shard_map/all_gather | solution.py:22
  198.6 4.8 fusion.2
  203.4 87.9 %all-gather.9.cloned.1.call-done = bf16[2048,1408]{1,0:T(8,128)(2,1)} async-done(((bf16[256,1408]{1,0:T(8,128)(2,1)}), bf16[2048,1408]{1,0:T(8,128)(2,1)}) %all-gather.9.cloned.1.call-update) | async-done | bytes 5767184 | tf_op jit(solution)/shard_map/all_gather | solution.py:16
  291.3 4.9 multiply_convert_fusion
  296.2 0.0 all-gather.13.cloned.1.call-update
  296.2 0.0 all-gather.15.cloned.1.call-start
  296.3 0.5 all-gather.15.cloned.1.call-update
  296.8 0.0 all-gather.17.cloned.1.call-start
  296.8 0.5 all-gather.17.cloned.1.call-update
  297.4 27.9 %all_to_all.38 = bf16[128,8,256]{0,2,1:T(8,128)(2,1)S(1)} all-to-all(bf16[128,8,256]{0,2,1:T(8,128)(2,1)S(1)} %bitcast.26), channel_id=1, replica_groups=mesh['rep'=2,'fs'=8,'tp'=2] {'fs'}, dimensions={1} | all-to-all | bytes 1048576 | tf_op jit(solution)/shard_map/all_to_all | solution.py:43
  325.3 3.5 all-to-all-start.1
  328.8 0.0 all-reduce.3.cloned.1.call-start
  328.9 0.2 copy.15
  329.1 25.8 %all-to-all-done.1 = bf16[128,8,256]{0,2,1:T(8,128)(2,1)S(1)} async-done(((bf16[128,8,256]{0,2,1:T(8,128)(2,1)}), bf16[128,8,256]{0,2,1:T(8,128)(2,1)S(1)}, u32[]{:S(2)}, u32[]{:S(2)}) %all-to-all-start.1) | async-done | bytes 524320 | tf_op jit(solution)/shard_map/all_to_all | solution.py:44
  354.9 0.2 copy.16
  355.1 10.2 %all-gather.13.cloned.1.call-done = bf16[1024,1408]{1,0:T(8,128)(2,1)} async-done(((bf16[128,1408]{1,0:T(8,128)(2,1)}), bf16[1024,1408]{1,0:T(8,128)(2,1)}) %all-gather.13.cloned.1.call-update) | async-done | bytes 2883600 | tf_op jit(solution)/shard_map/all_gather | solution.py:48
  365.4 3.9 convolution_bitcast_fusion.1
  369.2 54.6 %all-gather.15.cloned.1.call-done = bf16[1024,1408]{1,0:T(8,128)(2,1)} async-done(((bf16[128,1408]{1,0:T(8,128)(2,1)}), bf16[1024,1408]{1,0:T(8,128)(2,1)}) %all-gather.15.cloned.1.call-update) | async-done | bytes 2883600 | tf_op jit(solution)/shard_map/all_gather | solution.py:54
  423.8 3.9 convolution_bitcast_fusion
  427.7 54.7 %all-gather.17.cloned.1.call-done = bf16[1024,1408]{1,0:T(8,128)(2,1)} async-done(((bf16[128,1408]{1,0:T(8,128)(2,1)}), bf16[1024,1408]{1,0:T(8,128)(2,1)}) %all-gather.17.cloned.1.call-update) | async-done | bytes 2883600 | tf_op jit(solution)/shard_map/all_gather | solution.py:59
  482.4 3.9 fusion.5
  486.3 0.0 copy-start
  486.3 0.0 all-reduce.3.cloned.1.call-update
  486.3 0.0 copy-start.1
  486.3 0.0 reduce-scatter.2.cloned.1.call-start
  486.4 0.9 copy-done
  487.3 4.6 fusion.4
  491.9 0.0 copy-done.1
  491.9 5.4 fusion
  497.3 0.0 reduce-scatter.2.cloned.1.call-update
  497.3 98.6 %all-reduce.3.cloned.1.call-done = (f32[256,1408]{0,1:T(8,128)}, f32[256,1408]{0,1:T(8,128)}, f32[1408,256]{1,0:T(8,128)}) async-done(((f32[256,1408]{0,1:T(8,128)}, f32[256,1408]{0,1:T(8,128)}, f32[1408,256]{1,0:T(8,128)}), (f32[256,1408]{0,1:T(8,128)}, f32[256,1408]{0,1:T(8,128)}, f32[1408,256]{1,0:T(8,128)})) %all-reduce.3.cloned.1.call-update) | async-done | bytes 4325392 | tf_op jit(solution)/shard_map/psum | solution.py:64
  595.9 0.0 copy-start.3
  595.9 0.0 copy-start.2
  595.9 3.0 copy.17
  598.9 0.0 copy-done.3
  598.9 1.5 copy.18
  600.5 6.2 %reduce-scatter.2.cloned.1.call-done = bf16[128,1024]{1,0:T(8,128)(2,1)} async-done(((bf16[128,2048]{1,0:T(8,128)(2,1)}), bf16[128,1024]{1,0:T(8,128)(2,1)}) %reduce-scatter.2.cloned.1.call-update) | async-done | bytes 262160 | tf_op jit(solution)/shard_map/reduce_scatter | solution.py:39
  606.6 0.0 copy-done.2
  606.6 1.1 copy.22
Async XLA Ops:
  7.2 98.1 %all-gather.11.cloned.1.call-start = ((), (), s32[]{:S(2)}) async-start(), calls=%async_computation.5 | async-start | bytes 6488064 | tf_op jit(solution)/shard_map/all_gather | solution.py:15
  7.9 190.7 %all-gather.7.cloned.1.call-start = ((), (), s32[]{:S(2)}) async-start(), calls=%async_computation.3 | async-start | bytes 6488064 | tf_op jit(solution)/shard_map/all_gather | solution.py:22
  8.6 282.7 %all-gather.9.cloned.1.call-start = ((), (), s32[]{:S(2)}) async-start(), calls=%async_computation.4 | async-start | bytes 6488064 | tf_op jit(solution)/shard_map/all_gather | solution.py:16
  9.4 356.0 %all-gather.13.cloned.1.call-start = ((), (), s32[]{:S(2)}) async-start(), calls=%async_computation.7 | async-start | bytes 3244032 | tf_op jit(solution)/shard_map/all_gather | solution.py:48
  296.2 127.6 %all-gather.15.cloned.1.call-start = ((), (), s32[]{:S(2)}) async-start(), calls=%async_computation.8 | async-start | bytes 3244032 | tf_op jit(solution)/shard_map/all_gather | solution.py:54
  296.8 185.6 %all-gather.17.cloned.1.call-start = ((), (), s32[]{:S(2)}) async-start(), calls=%async_computation.9 | async-start | bytes 3244032 | tf_op jit(solution)/shard_map/all_gather | solution.py:59
  325.3 29.6 %all-to-all-start.1 = ((bf16[128,8,256]{0,2,1:T(8,128)(2,1)}), bf16[128,8,256]{0,2,1:T(8,128)(2,1)S(1)}, u32[]{:S(2)}, u32[]{:S(2)}) async-start(bf16[128,8,256]{0,2,1:T(8,128)(2,1)} %bitcast.5), calls=%async_computation.2 | async-start | bytes 1048576 | tf_op jit(solution)/shard_map/all_to_all | solution.py:44
  328.8 267.0 %all-reduce.3.cloned.1.call-start = ((), (), s32[]{:S(2)}) async-start(), calls=%async_computation.10 | async-start | bytes 8650752 | tf_op jit(solution)/shard_map/psum | solution.py:64
  486.3 1.0 copy-start
  486.3 5.6 copy-start.1
  486.3 120.3 %reduce-scatter.2.cloned.1.call-start = ((), (), s32[]{:S(2)}) async-start(), calls=%async_computation.6 | async-start | bytes 786432 | tf_op jit(solution)/shard_map/reduce_scatter | solution.py:39
  595.9 3.1 copy-start.3
  595.9 10.8 %copy-start.2 = (f32[1408,256]{1,0:T(8,128)S(1)}, f32[1408,256]{1,0:T(8,128)}, u32[]{:S(2)}) copy-start(f32[1408,256]{1,0:T(8,128)} %get-tuple-element.25) | copy-start | bytes 4325380
Sparse Core Ops, SparseCore 0:
  10.2 95.0 all-gather.10
  107.3 91.2 all-gather.6
  200.8 90.4 all-gather.8
  296.3 68.9 all-gather.12
  367.4 56.4 all-gather.14
  426.4 55.9 all-gather.16
  486.4 109.3 all-reduce.2
  598.7 7.9 reduce-scatter.1
where the time goes:
time: 615 us
  waiting for transfers between devices  520 us (85%)
  matrix products  34.9 us (6%)
  blocking collectives  32.5 us (5%)
  between operations  14.2 us (2%)
  local copies, waits for them, and re-layouts  9.26 us (2%)
    psum x1, waiting for transfers between devices, per_device(): lax.psum((gate_grads, up_grads, down_grads), 'rep')  98.6 us
    all_gather x1, waiting for transfers between devices, per_device(): lax.all_gather(down_weight, 'fs', axis=1, tiled=True)  89.7 us
    all_gather x1, waiting for transfers between devices, per_device(): lax.all_gather(gate_weight, 'fs', axis=0, tiled=True)  88.9 us
    all_gather x1, waiting for transfers between devices, per_device(): lax.all_gather(up_weight, 'fs', axis=0, tiled=True)  87.9 us
    all_gather x1, waiting for transfers between devices, per_device(): lax.all_gather(hidden, 'fs', axis=0, tiled=True)  54.7 us
    all_gather x1, waiting for transfers between devices, per_device(): lax.all_gather(grad_up, 'fs', axis=0, tiled=True)  54.6 us
    all_to_all x1, blocking collectives, per_device(): lax.all_to_all(input_full, 'fs', split_axis=1, concat_axis=0, tiled=True)  27.9 us
    all_to_all x1, waiting for transfers between devices, per_device(): lax.all_to_all(cotan_full, 'fs', split_axis=1, concat_axis=0, tiled=True)  25.8 us
  transfers between devices with their start and end apart: 9, of which 9 were waited for; matrix products, arithmetic and copies ran while one was open for 5% of the time, Pallas kernels for 0%

commit v1 on v0

v1 whole, which is shorter than its diff:
```python
import functools

import jax
import jax.numpy as jnp
from jax import lax
from jax.experimental import pallas as pl
from jax.experimental.pallas import tpu as pltpu
from jax.sharding import PartitionSpec as P

MESH = pl.DeviceIdType.MESH


def enter(n_rep, n_fs, n_tp):
    barrier = pltpu.get_barrier_semaphore()
    for axis, n in (("rep", n_rep), ("fs", n_fs), ("tp", n_tp)):
        me = lax.axis_index(axis)
        for k in range(1, n):
            pl.semaphore_signal(
                barrier, inc=1, device_id={axis: lax.rem(me + k, n)}, device_id_type=MESH
            )
    pl.semaphore_wait(barrier, n_rep + n_fs + n_tp - 3)


class Sender:
    def __init__(self, sems):
        self.sems, self.used, self.pending = sems, 0, []

    def send(self, src, dst, recv_sem, axis, peer):
        copy = pltpu.make_async_remote_copy(
            src_ref=src,
            dst_ref=dst,
            send_sem=self.sems.at[self.used],
            recv_sem=recv_sem,
            device_id={axis: peer},
            device_id_type=MESH,
        )
        self.used += 1
        copy.start()
        self.pending.append(copy)

    def local(self, src, dst):
        copy = pltpu.make_async_copy(src, dst, self.sems.at[self.used])
        self.used += 1
        copy.start()
        self.pending.append(copy)

    def finish(self):
        for copy in self.pending:
            if hasattr(copy, "wait_send") and copy.is_remote:
                copy.wait_send()
            else:
                copy.wait()


def arrived(slot, recv_sem):
    pltpu.make_async_copy(slot, slot, recv_sem).wait()


def near_first(n):
    return sorted(range(1, n), key=lambda k: min(k, n - k))


def gather_kernel(
    sizes, x_ref, c_ref, w_ref, x_out, c_out, w_out, sends, act_recv, w_recv
):
    n_rep, n_fs, n_tp, n_y = sizes
    n_z = n_fs // n_y
    rep, fs, tp = (lax.axis_index(axis) for axis in ("rep", "fs", "tp"))
    z, y = fs // n_y, lax.rem(fs, n_y)
    width = x_ref.shape[1]
    depth = w_ref.shape[3]
    enter(n_rep, n_fs, n_tp)
    out = Sender(sends)
    acts = ((x_ref, x_out), (c_ref, c_out))

    def act_slot(a, owner, part):
        return acts[a][1].at[owner, :, pl.ds(pl.multiple_of(part * width, width), width)]

    def w_slot(half, owner):
        if depth % 128 == 0:
            return w_out.at[half, :, pl.ds(pl.multiple_of(owner * depth, depth), depth)]
        return w_out.at[half, owner]

    def to_tp(a, owner, src):
        for k in range(1, n_tp):
            out.send(
                src, act_slot(a, owner, tp), act_recv.at[a, owner, tp], "tp", lax.rem(tp + k, n_tp)
            )

    def to_y(a, owner, src):
        for k in range(1, n_y):
            peer = z * n_y + lax.rem(y + k, n_y)
            out.send(src, act_slot(a, owner, tp), act_recv.at[a, owner, tp], "fs", peer)

    for a in range(2):
        src = acts[a][0]
        to_y(a, fs, src)
        for k in near_first(n_z):
            peer = lax.rem(z + k, n_z) * n_y + y
            out.send(src, act_slot(a, fs, tp), act_recv.at[a, fs, tp], "fs", peer)
    for k in near_first(n_fs):
        peer = lax.rem(fs + k, n_fs)
        out.send(w_ref.at[peer, rep], w_slot(rep, fs), w_recv.at[rep, fs], "fs", peer)
    for k in range(1, n_rep):
        out.send(
            w_ref.at[fs, rep], w_slot(rep, fs), w_recv.at[rep, fs], "rep", lax.rem(rep + k, n_rep)
        )
    for a in range(2):
        to_tp(a, fs, acts[a][0])
        out.local(acts[a][0], act_slot(a, fs, tp))
    out.local(w_ref.at[fs, rep], w_slot(rep, fs))

    for k in near_first(n_z):
        owner = lax.rem(z + n_z - k, n_z) * n_y + y
        for a in range(2):
            slot = act_slot(a, owner, tp)
            arrived(slot, act_recv.at[a, owner, tp])
            to_y(a, owner, slot)
            to_tp(a, owner, slot)
    for k in near_first(n_fs):
        owner = lax.rem(fs + n_fs - k, n_fs)
        slot = w_slot(rep, owner)
        arrived(slot, w_recv.at[rep, owner])
        for j in range(1, n_rep):
            out.send(slot, w_slot(rep, owner), w_recv.at[rep, owner], "rep", lax.rem(rep + j, n_rep))
    for kz in [0] + near_first(n_z):
        for ky in range(1, n_y):
            owner = lax.rem(z + n_z - kz, n_z) * n_y + lax.rem(y + ky, n_y)
            for a in range(2):
                slot = act_slot(a, owner, tp)
                arrived(slot, act_recv.at[a, owner, tp])
                to_tp(a, owner, slot)
    for j in range(1, n_rep):
        half = lax.rem(rep + j, n_rep)
        for k in range(n_fs):
            owner = lax.rem(fs + k, n_fs)
            arrived(w_slot(half, owner), w_recv.at[half, owner])
    for j in range(1, n_tp):
        part = lax.rem(tp + j, n_tp)
        for k in range(n_fs):
            owner = lax.rem(fs + k, n_fs)
            for a in range(2):
                arrived(act_slot(a, owner, part), act_recv.at[a, owner, part])
    out.finish()


def scatter_kernel(
    sizes, p_ref, g_ref, x_out, g_out,
    p_in, p_sum, g_in, g_sum, sends, p_recv, g_recv, x_recv, gx_recv,
):
    n_rep, n_fs, n_tp = sizes
    rep, fs, tp = (lax.axis_index(axis) for axis in ("rep", "fs", "tp"))
    rows, width = p_sum.shape[1:]
    enter(n_rep, n_fs, n_tp)
    out = Sender(sends)
    order = near_first(n_fs) + [0]

    def p_part(owner, part):
        return p_ref.at[owner, :, pl.ds(pl.multiple_of(part * width, width), width)]

    for k in order:
        owner = lax.rem(fs + k, n_fs)
        for j in range(1, n_tp):
            peer = lax.rem(tp + j, n_tp)
            out.send(p_part(owner, peer), p_in.at[j - 1, owner], p_recv.at[j - 1, owner], "tp", peer)
    for k in order:
        owner = lax.rem(fs + k, n_fs)
        for j in range(1, n_rep):
            peer = lax.rem(rep + j, n_rep)
            out.send(
                g_ref.at[owner, peer], g_in.at[j - 1, owner], g_recv.at[j - 1, owner], "rep", peer
            )
    for k in order:
        owner = lax.rem(fs + k, n_fs)
        total = p_part(owner, tp)[...].astype(jnp.float32)
        for j in range(n_tp - 1):
            arrived(p_in.at[j, owner], p_recv.at[j, owner])
            total = total + p_in[j, owner].astype(jnp.float32)
        p_sum[owner] = total.astype(jnp.bfloat16)
        if k:
            out.send(p_sum.at[owner], x_out.at[fs], x_recv.at[fs], "fs", owner)
        else:
            out.local(p_sum.at[owner], x_out.at[fs])
    for k in order:
        owner = lax.rem(fs + k, n_fs)
        total = g_ref[owner, rep].astype(jnp.float32)
        for j in range(n_rep - 1):
            arrived(g_in.at[j, owner], g_recv.at[j, owner])
            total = total + g_in[j, owner].astype(jnp.float32)
        g_sum[owner] = total.astype(jnp.bfloat16)
        slot = g_out.at[rep, fs]
        if k:
            out.send(g_sum.at[owner], slot, gx_recv.at[rep, fs], "fs", owner)
        else:
            out.local(g_sum.at[owner], slot)
            for j in range(1, n_rep):
                out.send(
                    g_sum.at[owner], slot, gx_recv.at[rep, fs], "rep", lax.rem(rep + j, n_rep)
                )
    for k in near_first(n_fs):
        owner = lax.rem(fs + n_fs - k, n_fs)
        slot = g_out.at[rep, owner]
        arrived(slot, gx_recv.at[rep, owner])
        for j in range(1, n_rep):
            out.send(slot, slot, gx_recv.at[rep, owner], "rep", lax.rem(rep + j, n_rep))
    for k in near_first(n_fs):
        owner = lax.rem(fs + n_fs - k, n_fs)
        arrived(x_out.at[owner], x_recv.at[owner])
    for j in range(1, n_rep):
        half = lax.rem(rep + j, n_rep)
        for k in range(n_fs):
            owner = lax.rem(fs + k, n_fs)
            arrived(g_out.at[half, owner], gx_recv.at[half, owner])
    out.finish()


VMEM = pl.BlockSpec(memory_space=pltpu.VMEM)
ANY = pl.BlockSpec(memory_space=pl.ANY)
DMA = pltpu.SemaphoreType.DMA


def per_device(n_rep, n_fs, n_tp, x, c, gate_weight, up_weight, down_weight):
    bf16, f32 = jnp.bfloat16, jnp.float32
    n_y = max(k for k in range(1, n_fs + 1) if n_fs % k == 0 and k * k <= n_fs)
    n_z = n_fs // n_y
    tokens, width = x.shape
    depth, hidden_tp = gate_weight.shape
    model = width * n_tp
    units = hidden_tp // n_fs
    step = 16 * n_rep
    rows = -(-3 * units // step) * step
    half = rows // n_rep

    w = jnp.concatenate(
        [
            gate_weight.T.reshape(n_fs, units, depth),
            up_weight.T.reshape(n_fs, units, depth),
            down_weight.reshape(n_fs, units, depth),
            jnp.zeros((n_fs, rows - 3 * units, depth), bf16),
        ],
        axis=1,
    ).reshape(n_fs, n_rep, half, depth)
    aligned = depth % 128 == 0
    w_shape = (n_rep, half, model) if aligned else (n_rep, n_fs, half, depth)
    n_sends = (
        2 * ((n_z - 1) + n_z * (n_y - 1) + n_fs * (n_tp - 1) + 1)
        + (n_fs - 1) + n_fs * (n_rep - 1) + 1
    )
    x_all, c_all, w_all = pl.pallas_call(
        functools.partial(gather_kernel, (n_rep, n_fs, n_tp, n_y)),
        out_shape=(
            jax.ShapeDtypeStruct((n_fs, tokens, model), bf16),
            jax.ShapeDtypeStruct((n_fs, tokens, model), bf16),
            jax.ShapeDtypeStruct(w_shape, bf16),
        ),
        in_specs=[VMEM] * 3,
        out_specs=(ANY,) * 3,
        scratch_shapes=[DMA((n_sends,)), DMA((2, n_fs, n_tp)), DMA((n_rep, n_fs))],
        compiler_params=pltpu.CompilerParams(collective_id=0, has_side_effects=True),
    )(x, c, w)
    x_all, c_all = (v.reshape(n_fs * tokens, model) for v in (x_all, c_all))
    if not aligned:
        w_all = w_all.transpose(0, 2, 1, 3)
    w_all = w_all.reshape(rows, model)
    w_in, w_down = w_all[: 2 * units], w_all[2 * units : 3 * units]

    last = (((1,), (1,)), ((), ()))
    first = (((0,), (0,)), ((), ()))
    pre = lax.dot_general(x_all, w_in, last, preferred_element_type=f32)
    grad_hidden = lax.dot_general(c_all, w_down, last, preferred_element_type=f32)
    gate_pre, up_pre = pre[:, :units], pre[:, units:]
    sigmoid_gate = jax.nn.sigmoid(gate_pre)
    activated = gate_pre * sigmoid_gate
    hidden = (activated * up_pre).astype(bf16)
    grad_gate = (
        grad_hidden * up_pre * sigmoid_gate * (1.0 + gate_pre * (1.0 - sigmoid_gate))
    ).astype(bf16)
    grad_up = (grad_hidden * activated).astype(bf16)
    grads = jnp.concatenate([grad_gate, grad_up], axis=1)
    partial = jnp.dot(grads, w_in, preferred_element_type=f32).astype(bf16)
    partial = partial.reshape(n_fs, tokens, model)
    g = jnp.concatenate(
        [
            lax.dot_general(grads, x_all, first, preferred_element_type=f32).astype(bf16),
            lax.dot_general(hidden, c_all, first, preferred_element_type=f32).astype(bf16),
            jnp.zeros((rows - 3 * units, model), bf16),
        ],
        axis=0,
    )
    g = g.reshape(n_rep, half, n_fs, depth).transpose(2, 0, 1, 3)
    n_sends = n_fs * (n_tp - 1) + n_fs * (n_rep - 1) + n_fs + n_fs + n_fs * (n_rep - 1)
    dx, dw = pl.pallas_call(
        functools.partial(scatter_kernel, (n_rep, n_fs, n_tp)),
        out_shape=(
            jax.ShapeDtypeStruct((n_fs, tokens, width), bf16),
            jax.ShapeDtypeStruct((n_rep, n_fs, half, depth), bf16),
        ),
        in_specs=[VMEM] * 2,
        out_specs=(ANY,) * 2,
        scratch_shapes=[
            pltpu.VMEM((n_tp - 1, n_fs, tokens, width), bf16),
            pltpu.VMEM((n_fs, tokens, width), bf16),
            pltpu.VMEM((n_rep - 1, n_fs, half, depth), bf16),
            pltpu.VMEM((n_fs, half, depth), bf16),
            DMA((n_sends,)),
            DMA((n_tp - 1, n_fs)),
            DMA((n_rep - 1, n_fs)),
            DMA((n_fs,)),
            DMA((n_rep, n_fs)),
        ],
        compiler_params=pltpu.CompilerParams(collective_id=1, has_side_effects=True),
    )(partial, g)
    grad_inputs = jnp.sum(dx.astype(f32), axis=0).astype(bf16)
    dw = dw.transpose(1, 0, 2, 3).reshape(n_fs, rows, depth)
    gate_grads, up_grads, down_grads = (
        dw[:, i * units : (i + 1) * units].reshape(hidden_tp, depth) for i in range(3)
    )
    return (
        grad_inputs,
        gate_grads.T.astype(f32),
        up_grads.T.astype(f32),
        down_grads.astype(f32),
    )


def solution(mesh):
    n_rep, n_fs, n_tp = (mesh.shape[axis] for axis in ("rep", "fs", "tp"))
    placed = (
        P(("rep", "fs"), "tp"),
        P(("rep", "fs"), "tp"),
        P("fs", "tp"),
        P("fs", "tp"),
        P("tp", "fs"),
    )
    return jax.shard_map(
        functools.partial(per_device, n_rep, n_fs, n_tp),
        mesh=mesh,
        in_specs=placed,
        out_specs=(P(("rep", "fs"), "tp"), P("fs", "tp"), P("fs", "tp"), P("tp", "fs")),
        check_vma=False,
    )
```

time: 615 us -> 212 us (0.34)
  the two profiles are of different devices: /device:TPU:0 before, /device:TPU:16 now
where the time goes in v1:
time: 212 us
  Pallas kernels  181 us (85%)
  matrix products  13.2 us (6%)
  local copies, waits for them, and re-layouts  9.93 us (5%)
  other arithmetic  6.69 us (3%)
    pallas_call x1, Pallas kernels, per_device(): pl.pallas_call(functools.partial(scatter_kernel, (n_rep, n_fs, n_tp)), ou...  91.6 us
    pallas_call x1, Pallas kernels, per_device(): pl.pallas_call(functools.partial(gather_kernel, (n_rep, n_fs, n_tp, n_y))...  89.7 us
    unnamed x15, local copies, waits for them, and re-layouts  7.73 us
    dot_general x1, matrix products, per_device(): pre = lax.dot_general(x_all, w_in, last, preferred_element_type=f32)  4.46 us
    dot_general x1, matrix products, per_device(): partial = jnp.dot(grads, w_in, preferred_element_type=f32).astype(bf16)  4.33 us

profile of v1, /device:TPU:16, one launch (start us, length us, event | category | flops | bytes accessed | tf_op | source)
XLA Modules:
  0.0 211.8 jit_solution(9741239074097474222)
XLA Ops:
  0.6 0.0 copy-start.1
  0.7 0.1 pad.8.clone
  0.7 1.4 copy.13
  2.2 1.4 copy.14
  3.5 0.0 copy-done.1
  3.6 1.8 maximum_maximum_fusion
  5.4 89.7 %shard_map.84 = (bf16[8,128,2048]{2,1,0:T(8,128)(2,1)}, bf16[8,128,2048]{2,1,0:T(8,128)(2,1)}, bf16[2,272,2048]{2,1,0:T(8,128)(2,1)}) custom-call(bf16[128,1024]{1,0:T(8,128)(2,1)} %x_ref.1, bf16[128,1024]{1,0:T(8,128)(2,1)} %c_ref.1, bf16[8,2,272,256]{3,2,1,0:T(8,128)(2,1)} %bitcast.39), custom_call_target="tpu_custom_call" | custom-call | tf_op jit(solution)/shard_map/pallas_call | solution.py:249
  95.1 0.0 copy-start.3
  95.1 4.5 %fusion.1 = f32[1024,352]{0,1:T(8,128)S(1)} fusion(bf16[1024,2048]{1,0:T(8,128)(2,1)} %bitcast.47, bf16[544,2048]{1,0:T(8,128)(2,1)} %bitcast.51), kind=kOutput, calls=%fused_computation.9 | convolution fusion | flops 1476395008 | bytes 7077888 | tf_op jit(solution)/shard_map/dot_general | solution.py:269
  99.6 0.0 copy-done.3
  99.6 0.0 copy-start.4
  99.6 1.0 convolution_convert_fusion.2
  100.6 0.7 copy-done.4
  101.2 0.0 copy-start.2
  101.2 1.7 multiply_convert_fusion.2
  103.0 0.5 copy-done.2
  103.4 1.7 convolution_convert_fusion.1
  105.1 0.4 maximum_maximum_fusion.1
  105.5 0.7 copy.19
  106.3 1.8 copy.21
  108.1 4.3 %convolution_convert_fusion = bf16[1024,2048]{1,0:T(8,128)(2,1)} fusion(bf16[544,2048]{1,0:T(8,128)(2,1)S(1)} %bitcast.53, bf16[1024,176]{0,1:T(8,128)(2,1)S(1)} %get-tuple-element.22, bf16[1024,176]{0,1:T(8,128)(2,1)S(1)} %get-tuple-element.21), kind=kOutput, calls=%fused_computation | convolution fusion | flops 1479933952 | bytes 6356992 | tf_op jit(solution)/shard_map/dot_general | solution.py:280
  112.4 91.6 %shard_map.85 = (bf16[8,128,1024]{2,1,0:T(8,128)(2,1)}, bf16[2,8,272,256]{3,2,1,0:T(8,128)(2,1)}) custom-call(bf16[8,128,2048]{2,1,0:T(8,128)(2,1)} %bitcast.42, bf16[8,2,272,256]{3,2,1,0:T(8,128)(2,1)} %bitcast.37), custom_call_target="tpu_custom_call" | custom-call | tf_op jit(solution)/shard_map/pallas_call | solution.py:292
  204.0 0.0 copy-start
  204.0 2.9 %reduce_sum.12 = bf16[128,1024]{1,0:T(8,128)(2,1)} reduce(bf16[8,128,1024]{2,1,0:T(8,128)(2,1)} %get-tuple-element.12, bf16[]{:T(256)} %constant.2.clone.1), dimensions={0}, to_apply=%region_0.0 | reduce | flops 917504 | bytes 2359298 | tf_op jit(solution)/shard_map/reduce_sum | solution.py:313
  206.9 0.0 copy-done
  206.9 0.1 copy.16
  207.0 0.1 fusion.10
  207.2 1.3 bitcast_convert_fusion
  208.4 0.3 convert_bitcast_fusion
  208.8 1.5 copy.18
  210.3 1.5 copy.17
  (1 shorter events, 0.0 us)
Async XLA Ops:
  0.6 2.9 %copy-start.1 = (bf16[1408,256]{1,0:T(8,128)(2,1)S(1)}, bf16[1408,256]{1,0:T(8,128)(2,1)}, u32[]{:S(2)}) copy-start(bf16[1408,256]{1,0:T(8,128)(2,1)} %param.9) | copy-start | bytes 2162692
  95.1 4.5 %copy-start.3 = (bf16[8,128,2048]{2,1,0:T(8,128)(2,1)S(1)}, bf16[8,128,2048]{2,1,0:T(8,128)(2,1)}, u32[]{:S(2)}) copy-start(bf16[8,128,2048]{2,1,0:T(8,128)(2,1)} %get-tuple-element.9) | copy-start | bytes 12582916
  99.6 1.6 copy-start.4
  101.2 2.2 %copy-start.2 = (bf16[8,128,2048]{2,1,0:T(8,128)(2,1)S(1)}, bf16[8,128,2048]{2,1,0:T(8,128)(2,1)}, u32[]{:S(2)}) copy-start(bf16[8,128,2048]{2,1,0:T(8,128)(2,1)} %get-tuple-element.11) | copy-start | bytes 12582916
  204.0 2.9 %copy-start = (bf16[2,8,272,256]{3,2,1,0:T(8,128)(2,1)S(1)}, bf16[2,8,272,256]{3,2,1,0:T(8,128)(2,1)}, u32[]{:S(2)}) copy-start(bf16[2,8,272,256]{3,2,1,0:T(8,128)(2,1)} %get-tuple-element.13) | copy-start | bytes 6684676

commit v2 on v1

--- a/solution.py
+++ b/solution.py
@@ -25,35 +25,51 @@
     def __init__(self, sems):
         self.sems, self.used, self.pending = sems, 0, []
 
-    def send(self, src, dst, recv_sem, axis, peer):
-        copy = pltpu.make_async_remote_copy(
-            src_ref=src,
-            dst_ref=dst,
-            send_sem=self.sems.at[self.used],
-            recv_sem=recv_sem,
-            device_id={axis: peer},
-            device_id_type=MESH,
-        )
+    def run(self, build, when):
+        if when is None:
+            build().start()
+        else:
+            pl.when(when)(lambda: build().start())
+
+    def send(self, src, dst, recv_sem, axis, peer, when=None):
+        def build(at=self.used):
+            return pltpu.make_async_remote_copy(
+                src_ref=src,
+                dst_ref=dst,
+                send_sem=self.sems.at[at],
+                recv_sem=recv_sem,
+                device_id={axis: peer},
+                device_id_type=MESH,
+            )
+
         self.used += 1
-        copy.start()
-        self.pending.append(copy)
+        self.run(build, when)
+        self.pending.append((lambda: build().wait_send(), when))
 
     def local(self, src, dst):
-        copy = pltpu.make_async_copy(src, dst, self.sems.at[self.used])
+        def build(at=self.used):
+            return pltpu.make_async_copy(src, dst, self.sems.at[at])
+
         self.used += 1
-        copy.start()
-        self.pending.append(copy)
+        self.run(build, None)
+        self.pending.append((lambda: build().wait(), None))
 
     def finish(self):
-        for copy in self.pending:
-            if hasattr(copy, "wait_send") and copy.is_remote:
-                copy.wait_send()
+        for wait, when in self.pending:
+            if when is None:
+                wait()
             else:
-                copy.wait()
-
-
-def arrived(slot, recv_sem):
-    pltpu.make_async_copy(slot, slot, recv_sem).wait()
+                pl.when(when)(wait)
+
+
+def arrived(slot, recv_sem, when=None):
+    def wait():
+        pltpu.make_async_copy(slot, slot, recv_sem).wait()
+
+    if when is None:
+        wait()
+    else:
+        pl.when(when)(wait)
 
 
 def near_first(n):
@@ -81,23 +97,22 @@
             return w_out.at[half, :, pl.ds(pl.multiple_of(owner * depth, depth), depth)]
         return w_out.at[half, owner]
 
-    def to_tp(a, owner, src):
+    def act_send(a, owner, src, axis, peer, when=None):
+        out.send(src, act_slot(a, owner, tp), act_recv.at[a, owner, tp], axis, peer, when)
+
+    def to_tp(a, owner, src, when=None):
         for k in range(1, n_tp):
-            out.send(
-                src, act_slot(a, owner, tp), act_recv.at[a, owner, tp], "tp", lax.rem(tp + k, n_tp)
-            )
-
-    def to_y(a, owner, src):
+            act_send(a, owner, src, "tp", lax.rem(tp + k, n_tp), when)
+
+    def to_y(a, owner, src, when=None):
         for k in range(1, n_y):
-            peer = z * n_y + lax.rem(y + k, n_y)
-            out.send(src, act_slot(a, owner, tp), act_recv.at[a, owner, tp], "fs", peer)
+            act_send(a, owner, src, "fs", z * n_y + lax.rem(y + k, n_y), when)
 
     for a in range(2):
         src = acts[a][0]
         to_y(a, fs, src)
-        for k in near_first(n_z):
-            peer = lax.rem(z + k, n_z) * n_y + y
-            out.send(src, act_slot(a, fs, tp), act_recv.at[a, fs, tp], "fs", peer)
+        act_send(a, fs, src, "fs", fs + n_y, z + 1 < n_z)
+        act_send(a, fs, src, "fs", fs - n_y, z >= 1)
     for k in near_first(n_fs):
         peer = lax.rem(fs + k, n_fs)
         out.send(w_ref.at[peer, rep], w_slot(rep, fs), w_recv.at[rep, fs], "fs", peer)
@@ -110,19 +125,33 @@
         out.local(acts[a][0], act_slot(a, fs, tp))
     out.local(w_ref.at[fs, rep], w_slot(rep, fs))
 
-    for k in near_first(n_z):
-        owner = lax.rem(z + n_z - k, n_z) * n_y + y
+    def swap_weights():
+        for k in near_first(n_fs):
+            owner = lax.rem(fs + n_fs - k, n_fs)
+            slot = w_slot(rep, owner)
+            arrived(slot, w_recv.at[rep, owner])
+            for j in range(1, n_rep):
+                peer = lax.rem(rep + j, n_rep)
+                out.send(slot, slot, w_recv.at[rep, owner], "rep", peer)
+
+    for k in range(1, n_z):
+        if k == max(n_z - 1, 1):
+            swap_weights()
         for a in range(2):
-            slot = act_slot(a, owner, tp)
-            arrived(slot, act_recv.at[a, owner, tp])
-            to_y(a, owner, slot)
-            to_tp(a, owner, slot)
-    for k in near_first(n_fs):
-        owner = lax.rem(fs + n_fs - k, n_fs)
-        slot = w_slot(rep, owner)
-        arrived(slot, w_recv.at[rep, owner])
-        for j in range(1, n_rep):
-            out.send(slot, w_slot(rep, owner), w_recv.at[rep, owner], "rep", lax.rem(rep + j, n_rep))
+            for here, onward, step in (
+                (z >= k, z + 1 < n_z, -1), (z + k < n_z, z >= 1, 1)
+            ):
+                owner = fs + step * k * n_y
+                slot = act_slot(a, owner, tp)
+                arrived(slot, act_recv.at[a, owner, tp], here)
+                if k < n_z - 1:
+                    act_send(
+                        a, owner, slot, "fs", fs - step * n_y, jnp.logical_and(here, onward)
+                    )
+                to_y(a, owner, slot, here)
+                to_tp(a, owner, slot, here)
+    if n_z == 1:
+        swap_weights()
     for kz in [0] + near_first(n_z):
         for ky in range(1, n_y):
             owner = lax.rem(z + n_z - kz, n_z) * n_y + lax.rem(y + ky, n_y)
@@ -145,49 +174,68 @@
 
 
 def scatter_kernel(
-    sizes, p_ref, g_ref, x_out, g_out,
-    p_in, p_sum, g_in, g_sum, sends, p_recv, g_recv, x_recv, gx_recv,
+    sizes, d_ref, w_ref, g_ref, x_ref, g_out,
+    p, p_in, q, y_in, r, x_in, g_in, g_sum, sends, p_recv, y_recv, x_recv, g_recv, gx_recv,
 ):
-    n_rep, n_fs, n_tp = sizes
+    n_rep, n_fs, n_tp, n_y = sizes
+    n_z = n_fs // n_y
+    f32, bf16 = jnp.float32, jnp.bfloat16
     rep, fs, tp = (lax.axis_index(axis) for axis in ("rep", "fs", "tp"))
-    rows, width = p_sum.shape[1:]
+    z, y = fs // n_y, lax.rem(fs, n_y)
+    rows, width = x_ref.shape
+    depth = g_sum.shape[2]
     enter(n_rep, n_fs, n_tp)
     out = Sender(sends)
     order = near_first(n_fs) + [0]
-
-    def p_part(owner, part):
-        return p_ref.at[owner, :, pl.ds(pl.multiple_of(part * width, width), width)]
-
-    for k in order:
-        owner = lax.rem(fs + k, n_fs)
-        for j in range(1, n_tp):
-            peer = lax.rem(tp + j, n_tp)
-            out.send(p_part(owner, peer), p_in.at[j - 1, owner], p_recv.at[j - 1, owner], "tp", peer)
+    zs = near_first(n_z) + [0]
+
+    def columns(part, size):
+        return pl.ds(pl.multiple_of(part * size, size), size)
+
+    def g_part(owner, half):
+        if depth % 128 == 0:
+            return g_ref.at[half, :, columns(owner, depth)]
+        return g_ref.at[half, owner]
+
     for k in order:
         owner = lax.rem(fs + k, n_fs)
         for j in range(1, n_rep):
             peer = lax.rem(rep + j, n_rep)
             out.send(
-                g_ref.at[owner, peer], g_in.at[j - 1, owner], g_recv.at[j - 1, owner], "rep", peer
+                g_part(owner, peer), g_in.at[j - 1, owner], g_recv.at[j - 1, owner], "rep", peer
             )
-    for k in order:
-        owner = lax.rem(fs + k, n_fs)
-        total = p_part(owner, tp)[...].astype(jnp.float32)
+    blocks = [(kz, ky) for ky in list(range(1, n_y)) + [0] for kz in zs]
+
+    def owner_of(kz, ky):
+        return lax.rem(z + kz, n_z) * n_y + lax.rem(y + ky, n_y)
+
+    for block in blocks:
+        owner = owner_of(*block)
+        p[owner] = jnp.dot(d_ref[owner], w_ref[...], preferred_element_type=f32).astype(bf16)
+        for j in range(1, n_tp):
+            peer = lax.rem(tp + j, n_tp)
+            out.send(
+                p.at[owner, :, columns(peer, width)],
+                p_in.at[j - 1, owner],
+                p_recv.at[j - 1, owner],
+                "tp",
+                peer,
+            )
+
+    def pair_sum(owner):
+        total = p[owner, :, columns(tp, width)].astype(f32)
         for j in range(n_tp - 1):
             arrived(p_in.at[j, owner], p_recv.at[j, owner])
-            total = total + p_in[j, owner].astype(jnp.float32)
-        p_sum[owner] = total.astype(jnp.bfloat16)
-        if k:
-            out.send(p_sum.at[owner], x_out.at[fs], x_recv.at[fs], "fs", owner)
-        else:
-            out.local(p_sum.at[owner], x_out.at[fs])
-    for k in order:
+            total = total + p_in[j, owner].astype(f32)
+        return total
+
+    def g_step(k):
         owner = lax.rem(fs + k, n_fs)
-        total = g_ref[owner, rep].astype(jnp.float32)
+        total = g_part(owner, rep)[...].astype(f32)
         for j in range(n_rep - 1):
             arrived(g_in.at[j, owner], g_recv.at[j, owner])
-            total = total + g_in[j, owner].astype(jnp.float32)
-        g_sum[owner] = total.astype(jnp.bfloat16)
+            total = total + g_in[j, owner].astype(f32)
+        g_sum[owner] = total.astype(bf16)
         slot = g_out.at[rep, fs]
         if k:
             out.send(g_sum.at[owner], slot, gx_recv.at[rep, fs], "fs", owner)
@@ -197,15 +245,47 @@
                 out.send(
                     g_sum.at[owner], slot, gx_recv.at[rep, fs], "rep", lax.rem(rep + j, n_rep)
                 )
+
+    for kz, ky in blocks:
+        if ky:
+            owner = owner_of(kz, ky)
+            q[owner] = pair_sum(owner).astype(bf16)
+            at = (ky - 1, lax.rem(z + kz, n_z))
+            out.send(
+                q.at[owner], y_in.at[at], y_recv.at[at], "fs", z * n_y + lax.rem(y + ky, n_y)
+            )
+    early = len(order) // 2
+    for k in order[:early]:
+        g_step(k)
+    for kz in zs:
+        owner = owner_of(kz, 0)
+        z_to = lax.rem(z + kz, n_z)
+        total = pair_sum(owner)
+        for ky in range(1, n_y):
+            at = (ky - 1, z_to)
+            arrived(y_in.at[at], y_recv.at[at])
+            total = total + y_in[at].astype(f32)
+        if kz:
+            r[z_to] = total.astype(bf16)
+            out.send(r.at[z_to], x_in.at[z], x_recv.at[z], "fs", owner)
+        else:
+            own = total
+            x_in[z] = own.astype(bf16)
+    for k in order[early:]:
+        g_step(k)
     for k in near_first(n_fs):
         owner = lax.rem(fs + n_fs - k, n_fs)
         slot = g_out.at[rep, owner]
         arrived(slot, gx_recv.at[rep, owner])
         for j in range(1, n_rep):
             out.send(slot, slot, gx_recv.at[rep, owner], "rep", lax.rem(rep + j, n_rep))
-    for k in near_first(n_fs):
-        owner = lax.rem(fs + n_fs - k, n_fs)
-        arrived(x_out.at[owner], x_recv.at[owner])
+    for kz in near_first(n_z):
+        z_from = lax.rem(z + n_z - kz, n_z)
+        arrived(x_in.at[z_from], x_recv.at[z_from])
+    total = x_in[0].astype(f32)
+    for k in range(1, n_z):
+        total = total + x_in[k].astype(f32)
+    x_ref[...] = total.astype(bf16)
     for j in range(1, n_rep):
         half = lax.rem(rep + j, n_rep)
         for k in range(n_fs):
@@ -243,7 +323,7 @@
     aligned = depth % 128 == 0
     w_shape = (n_rep, half, model) if aligned else (n_rep, n_fs, half, depth)
     n_sends = (
-        2 * ((n_z - 1) + n_z * (n_y - 1) + n_fs * (n_tp - 1) + 1)
+        2 * (2 + (2 * n_z - 1) * (n_y - 1) + (2 * n_z - 1) * (n_tp - 1) + 2 * n_z + n_fs * (n_tp - 1) + 1)
         + (n_fs - 1) + n_fs * (n_rep - 1) + 1
     )
     x_all, c_all, w_all = pl.pallas_call(
@@ -277,8 +357,6 @@
     ).astype(bf16)
     grad_up = (grad_hidden * activated).astype(bf16)
     grads = jnp.concatenate([grad_gate, grad_up], axis=1)
-    partial = jnp.dot(grads, w_in, preferred_element_type=f32).astype(bf16)
-    partial = partial.reshape(n_fs, tokens, model)
     g = jnp.concatenate(
         [
             lax.dot_general(grads, x_all, first, preferred_element_type=f32).astype(bf16),
@@ -287,30 +365,38 @@
         ],
         axis=0,
     )
-    g = g.reshape(n_rep, half, n_fs, depth).transpose(2, 0, 1, 3)
-    n_sends = n_fs * (n_tp - 1) + n_fs * (n_rep - 1) + n_fs + n_fs + n_fs * (n_rep - 1)
-    dx, dw = pl.pallas_call(
-        functools.partial(scatter_kernel, (n_rep, n_fs, n_tp)),
+    g = g.reshape(w_shape if aligned else (n_rep, half, n_fs, depth))
+    if not aligned:
+        g = g.transpose(0, 2, 1, 3)
+    n_sends = n_fs * (n_tp - 1) + 2 * n_fs * (n_rep - 1) + 3 * n_fs
+    grad_inputs, dw = pl.pallas_call(
+        functools.partial(scatter_kernel, (n_rep, n_fs, n_tp, n_y)),
         out_shape=(
-            jax.ShapeDtypeStruct((n_fs, tokens, width), bf16),
+            jax.ShapeDtypeStruct((tokens, width), bf16),
             jax.ShapeDtypeStruct((n_rep, n_fs, half, depth), bf16),
         ),
-        in_specs=[VMEM] * 2,
-        out_specs=(ANY,) * 2,
+        in_specs=[VMEM] * 3,
+        out_specs=(VMEM, ANY),
         scratch_shapes=[
+            pltpu.VMEM((n_fs, tokens, model), bf16),
             pltpu.VMEM((n_tp - 1, n_fs, tokens, width), bf16),
             pltpu.VMEM((n_fs, tokens, width), bf16),
+            pltpu.VMEM((n_y - 1, n_z, tokens, width), bf16),
+            pltpu.VMEM((n_z, tokens, width), bf16),
+            pltpu.VMEM((n_z, tokens, width), bf16),
             pltpu.VMEM((n_rep - 1, n_fs, half, depth), bf16),
             pltpu.VMEM((n_fs, half, depth), bf16),
             DMA((n_sends,)),
             DMA((n_tp - 1, n_fs)),
+            DMA((n_y - 1, n_z)),
+            DMA((n_z,)),
             DMA((n_rep - 1, n_fs)),
-            DMA((n_fs,)),
             DMA((n_rep, n_fs)),
         ],
-        compiler_params=pltpu.CompilerParams(collective_id=1, has_side_effects=True),
-    )(partial, g)
-    grad_inputs = jnp.sum(dx.astype(f32), axis=0).astype(bf16)
+        compiler_params=pltpu.CompilerParams(
+            collective_id=1, has_side_effects=True, vmem_limit_bytes=60 * 2**20
+        ),
+    )(grads.reshape(n_fs, tokens, 2 * units), w_in, g)
     dw = dw.transpose(1, 0, 2, 3).reshape(n_fs, rows, depth)
     gate_grads, up_grads, down_grads = (
         dw[:, i * units : (i + 1) * units].reshape(hidden_tp, depth) for i in range(3)

time: 212 us -> 173 us (0.82)
  the two profiles are of different devices: /device:TPU:16 before, /device:TPU:0 now
where the time goes in v2:
time: 173 us
  Pallas kernels  146 us (84%)
  local copies, waits for them, and re-layouts  11.6 us (7%)
  matrix products  8.74 us (5%)
  other arithmetic  5.26 us (3%)
    pallas_call x1, Pallas kernels, per_device(): pl.pallas_call(functools.partial(gather_kernel, (n_rep, n_fs, n_tp, n_y))...  73.1 us
    pallas_call x1, Pallas kernels, per_device(): pl.pallas_call(functools.partial(scatter_kernel, (n_rep, n_fs, n_tp, n_y)...  73 us
    unnamed x15, local copies, waits for them, and re-layouts  7.27 us
    dot_general x1, matrix products, per_device(): pre = lax.dot_general(x_all, w_in, last, preferred_element_type=f32)  4.46 us

profile of v2, /device:TPU:0, one launch (start us, length us, event | category | flops | bytes accessed | tf_op | source)
XLA Modules:
  0.0 172.5 jit_solution(6371992655614296705)
XLA Ops:
  0.6 0.0 copy-start.1
  0.7 0.1 pad.8.clone
  0.7 1.4 copy.14
  2.2 1.4 copy.15
  3.5 0.0 copy-done.1
  3.6 1.8 %maximum_maximum_fusion = bf16[8,544,256]{2,1,0:T(8,128)(2,1)} fusion(bf16[8,176,256]{2,1,0:T(8,128)(2,1)S(1)} %bitcast.42, bf16[8,176,256]{2,1,0:T(8,128)(2,1)S(1)} %bitcast.37, bf16[8,176,256]{2,1,0:T(8,128)(2,1)S(1)} %bitcast.36, bf16[544]{0:T(1024)(128)(2,1)S(1)} %pad.8.clone), kind=kLoop, calls=%fused_computation.2 | loop fusion | flops 8912896 | bytes 4392000 | tf_op jit(solution)/shard_map/concatenate | solution.py:314
  5.4 73.1 %shard_map.84 = (bf16[8,128,2048]{2,1,0:T(8,128)(2,1)}, bf16[8,128,2048]{2,1,0:T(8,128)(2,1)}, bf16[2,272,2048]{2,1,0:T(8,128)(2,1)}) custom-call(bf16[128,1024]{1,0:T(8,128)(2,1)} %x_ref.1, bf16[128,1024]{1,0:T(8,128)(2,1)} %c_ref.1, bf16[8,2,272,256]{3,2,1,0:T(8,128)(2,1)} %bitcast.33), custom_call_target="tpu_custom_call" | custom-call | tf_op jit(solution)/shard_map/pallas_call | solution.py:329
  78.5 0.0 copy-start.4
  78.5 4.5 %fusion.5 = f32[1024,352]{0,1:T(8,128)S(1)} fusion(bf16[1024,2048]{1,0:T(8,128)(2,1)} %bitcast.43, bf16[544,2048]{1,0:T(8,128)(2,1)} %bitcast.39), kind=kOutput, calls=%fused_computation.16 | convolution fusion | flops 1476395008 | bytes 7077888 | tf_op jit(solution)/shard_map/dot_general | solution.py:349
  83.0 0.0 copy-done.4
  83.0 0.0 copy-start
  83.0 0.9 convolution_convert_fusion.1
  83.9 0.7 copy-done
  84.6 0.0 copy-start.3
  84.6 1.7 multiply_convert_fusion.2
  86.3 1.2 slice.29.w_ref
  87.5 0.0 copy-done.3
  87.5 1.7 convolution_convert_fusion
  89.2 1.8 %maximum_maximum_fusion.1 = bf16[544,2048]{1,0:T(8,128)(2,1)} fusion(bf16[176,2048]{1,0:T(8,128)(2,1)S(1)} %convolution_convert_fusion.1, bf16[352,2048]{1,0:T(8,128)(2,1)S(1)} %convolution_convert_fusion, bf16[544]{0:T(1024)(128)(2,1)S(1)} %pad.8.clone), kind=kLoop, calls=%fused_computation.3 | loop fusion | flops 6684672 | bytes 4392000 | tf_op jit(solution)/shard_map/concatenate | solution.py:360
  91.0 1.2 copy.16
  92.2 73.0 %shard_map.85 = (bf16[128,1024]{1,0:T(8,128)(2,1)}, bf16[2,8,272,256]{3,2,1,0:T(8,128)(2,1)}) custom-call(bf16[8,128,352]{2,1,0:T(8,128)(2,1)} %bitcast.35, bf16[352,2048]{1,0:T(8,128)(2,1)} %slice.29.w_ref, bf16[2,272,2048]{2,1,0:T(8,128)(2,1)} %bitcast.32), custom_call_target="tpu_custom_call" | custom-call | tf_op jit(solution)/shard_map/pallas_call | solution.py:372
  165.2 1.8 %copy.17 = bf16[8,2,272,256]{3,2,1,0:T(8,128)(2,1)S(1)} copy(bf16[8,2,272,256]{3,2,0,1:T(8,128)(2,1)} %bitcast.38) | data formatting | bytes 4456448 | tf_op jit(solution)/shard_map/transpose | solution.py:400
  167.0 0.1 fusion.7
  167.2 1.3 bitcast_convert_fusion
  168.4 0.3 convert_bitcast_fusion
  168.7 0.0 copy-start.2
  168.7 1.5 copy.19
  170.3 1.5 copy.18
  171.8 0.0 copy-done.2
  171.8 0.7 copy.21
  (2 shorter events, 0.1 us)
Async XLA Ops:
  0.6 2.9 %copy-start.1 = (bf16[1408,256]{1,0:T(8,128)(2,1)S(1)}, bf16[1408,256]{1,0:T(8,128)(2,1)}, u32[]{:S(2)}) copy-start(bf16[1408,256]{1,0:T(8,128)(2,1)} %param.9) | copy-start | bytes 2162692
  78.5 4.5 %copy-start.4 = (bf16[8,128,2048]{2,1,0:T(8,128)(2,1)S(1)}, bf16[8,128,2048]{2,1,0:T(8,128)(2,1)}, u32[]{:S(2)}) copy-start(bf16[8,128,2048]{2,1,0:T(8,128)(2,1)} %get-tuple-element.9) | copy-start | bytes 12582916
  83.0 1.6 copy-start
  84.6 2.9 %copy-start.3 = (bf16[8,128,2048]{2,1,0:T(8,128)(2,1)S(1)}, bf16[8,128,2048]{2,1,0:T(8,128)(2,1)}, u32[]{:S(2)}) copy-start(bf16[8,128,2048]{2,1,0:T(8,128)(2,1)} %get-tuple-element.11) | copy-start | bytes 12582916
  168.7 3.1 %copy-start.2 = (bf16[128,1024]{1,0:T(8,128)(2,1)S(1)}, bf16[128,1024]{1,0:T(8,128)(2,1)}, u32[]{:S(2)}) copy-start(bf16[128,1024]{1,0:T(8,128)(2,1)} %get-tuple-element.29) | copy-start | bytes 786436

commit v3 on v2

--- a/solution.py
+++ b/solution.py
@@ -76,9 +76,27 @@
     return sorted(range(1, n), key=lambda k: min(k, n - k))
 
 
+def split_weights(weights, w_ref):
+    n_fs, n_rep, half, depth = w_ref.shape
+    units = weights[2].shape[0] // n_fs
+    turned = [weights[0][...].T, weights[1][...].T, weights[2][...]]
+    for owner in range(n_fs):
+        for i, value in enumerate(turned):
+            for h in range(n_rep):
+                low, high = max(i * units, h * half), min((i + 1) * units, (h + 1) * half)
+                if low < high:
+                    start = owner * units - i * units
+                    w_ref[owner, h, low - h * half : high - h * half] = value[
+                        start + low : start + high
+                    ]
+        used = 3 * units - (n_rep - 1) * half
+        w_ref[owner, n_rep - 1, used:] = jnp.zeros((half - used, depth), w_ref.dtype)
+
+
 def gather_kernel(
-    sizes, x_ref, c_ref, w_ref, x_out, c_out, w_out, sends, act_recv, w_recv
+    sizes, x_ref, c_ref, *refs
 ):
+    *weights, x_out, c_out, w_out, w_ref, sends, act_recv, w_recv = refs
     n_rep, n_fs, n_tp, n_y = sizes
     n_z = n_fs // n_y
     rep, fs, tp = (lax.axis_index(axis) for axis in ("rep", "fs", "tp"))
@@ -113,6 +131,13 @@
         to_y(a, fs, src)
         act_send(a, fs, src, "fs", fs + n_y, z + 1 < n_z)
         act_send(a, fs, src, "fs", fs - n_y, z >= 1)
+    for a in range(2):
+        to_tp(a, fs, acts[a][0])
+        out.local(acts[a][0], act_slot(a, fs, tp))
+    if len(weights) == 1:
+        w_ref = weights[0]
+    else:
+        split_weights(weights, w_ref)
     for k in near_first(n_fs):
         peer = lax.rem(fs + k, n_fs)
         out.send(w_ref.at[peer, rep], w_slot(rep, fs), w_recv.at[rep, fs], "fs", peer)
@@ -120,9 +145,6 @@
         out.send(
             w_ref.at[fs, rep], w_slot(rep, fs), w_recv.at[rep, fs], "rep", lax.rem(rep + k, n_rep)
         )
-    for a in range(2):
-        to_tp(a, fs, acts[a][0])
-        out.local(acts[a][0], act_slot(a, fs, tp))
     out.local(w_ref.at[fs, rep], w_slot(rep, fs))
 
     def swap_weights():
@@ -211,7 +233,9 @@
 
     for block in blocks:
         owner = owner_of(*block)
-        p[owner] = jnp.dot(d_ref[owner], w_ref[...], preferred_element_type=f32).astype(bf16)
+        p[owner] = jnp.dot(
+            d_ref[owner], w_ref[: d_ref.shape[2]], preferred_element_type=f32
+        ).astype(bf16)
         for j in range(1, n_tp):
             peer = lax.rem(tp + j, n_tp)
             out.send(
@@ -236,7 +260,7 @@
             arrived(g_in.at[j, owner], g_recv.at[j, owner])
             total = total + g_in[j, owner].astype(f32)
         g_sum[owner] = total.astype(bf16)
-        slot = g_out.at[rep, fs]
+        slot = g_out.at[fs, rep]
         if k:
             out.send(g_sum.at[owner], slot, gx_recv.at[rep, fs], "fs", owner)
         else:
@@ -254,10 +278,7 @@
             out.send(
                 q.at[owner], y_in.at[at], y_recv.at[at], "fs", z * n_y + lax.rem(y + ky, n_y)
             )
-    early = len(order) // 2
-    for k in order[:early]:
-        g_step(k)
-    for kz in zs:
+    def x_step(kz):
         owner = owner_of(kz, 0)
         z_to = lax.rem(z + kz, n_z)
         total = pair_sum(owner)
@@ -269,16 +290,25 @@
             r[z_to] = total.astype(bf16)
             out.send(r.at[z_to], x_in.at[z], x_recv.at[z], "fs", owner)
         else:
-            own = total
-            x_in[z] = own.astype(bf16)
-    for k in order[early:]:
-        g_step(k)
-    for k in near_first(n_fs):
-        owner = lax.rem(fs + n_fs - k, n_fs)
-        slot = g_out.at[rep, owner]
-        arrived(slot, gx_recv.at[rep, owner])
-        for j in range(1, n_rep):
-            out.send(slot, slot, gx_recv.at[rep, owner], "rep", lax.rem(rep + j, n_rep))
+            x_in[z] = total.astype(bf16)
+
+    def g_forward(k):
+        if k:
+            owner = lax.rem(fs + n_fs - k, n_fs)
+            slot = g_out.at[owner, rep]
+            arrived(slot, gx_recv.at[rep, owner])
+            for j in range(1, n_rep):
+                out.send(slot, slot, gx_recv.at[rep, owner], "rep", lax.rem(rep + j, n_rep))
+
+    for i, kz in enumerate(zs):
+        for k in order[i * n_y : (i + 1) * n_y]:
+            g_step(k)
+        x_step(kz)
+        if i:
+            for k in order[(i - 1) * n_y : i * n_y]:
+                g_forward(k)
+    for k in order[-n_y:]:
+        g_forward(k)
     for kz in near_first(n_z):
         z_from = lax.rem(z + n_z - kz, n_z)
         arrived(x_in.at[z_from], x_recv.at[z_from])
@@ -290,7 +320,7 @@
         half = lax.rem(rep + j, n_rep)
         for k in range(n_fs):
             owner = lax.rem(fs + k, n_fs)
-            arrived(g_out.at[half, owner], gx_recv.at[half, owner])
+            arrived(g_out.at[owner, half], gx_recv.at[half, owner])
     out.finish()
 
 
@@ -311,15 +341,12 @@
     rows = -(-3 * units // step) * step
     half = rows // n_rep
 
-    w = jnp.concatenate(
-        [
-            gate_weight.T.reshape(n_fs, units, depth),
-            up_weight.T.reshape(n_fs, units, depth),
-            down_weight.reshape(n_fs, units, depth),
-            jnp.zeros((n_fs, rows - 3 * units, depth), bf16),
-        ],
-        axis=1,
-    ).reshape(n_fs, n_rep, half, depth)
+    weights = [gate_weight, up_weight, down_weight]
+    if units % 16 or depth % 128 or 3 * units <= rows - half:
+        blocks = [gate_weight.T, up_weight.T, down_weight]
+        blocks = [v.reshape(n_fs, units, depth) for v in blocks]
+        blocks.append(jnp.zeros((n_fs, rows - 3 * units, depth), bf16))
+        weights = [jnp.concatenate(blocks, axis=1).reshape(n_fs, n_rep, half, depth)]
     aligned = depth % 128 == 0
     w_shape = (n_rep, half, model) if aligned else (n_rep, n_fs, half, depth)
     n_sends = (
@@ -333,11 +360,11 @@
             jax.ShapeDtypeStruct((n_fs, tokens, model), bf16),
             jax.ShapeDtypeStruct(w_shape, bf16),
         ),
-        in_specs=[VMEM] * 3,
+        in_specs=[VMEM] * (2 + len(weights)),
         out_specs=(ANY,) * 3,
-        scratch_shapes=[DMA((n_sends,)), DMA((2, n_fs, n_tp)), DMA((n_rep, n_fs))],
+        scratch_shapes=[pltpu.VMEM((n_fs, n_rep, half, depth), bf16), DMA((n_sends,)), DMA((2, n_fs, n_tp)), DMA((n_rep, n_fs))],
         compiler_params=pltpu.CompilerParams(collective_id=0, has_side_effects=True),
-    )(x, c, w)
+    )(x, c, *weights)
     x_all, c_all = (v.reshape(n_fs * tokens, model) for v in (x_all, c_all))
     if not aligned:
         w_all = w_all.transpose(0, 2, 1, 3)
@@ -373,7 +400,7 @@
         functools.partial(scatter_kernel, (n_rep, n_fs, n_tp, n_y)),
         out_shape=(
             jax.ShapeDtypeStruct((tokens, width), bf16),
-            jax.ShapeDtypeStruct((n_rep, n_fs, half, depth), bf16),
+            jax.ShapeDtypeStruct((n_fs, n_rep, half, depth), bf16),
         ),
         in_specs=[VMEM] * 3,
         out_specs=(VMEM, ANY),
@@ -396,8 +423,8 @@
         compiler_params=pltpu.CompilerParams(
             collective_id=1, has_side_effects=True, vmem_limit_bytes=60 * 2**20
         ),
-    )(grads.reshape(n_fs, tokens, 2 * units), w_in, g)
-    dw = dw.transpose(1, 0, 2, 3).reshape(n_fs, rows, depth)
+    )(grads.reshape(n_fs, tokens, 2 * units), w_all, g)
+    dw = dw.reshape(n_fs, rows, depth)
     gate_grads, up_grads, down_grads = (
         dw[:, i * units : (i + 1) * units].reshape(hidden_tp, depth) for i in range(3)
     )

time: 173 us -> 170 us (0.983)
  local copies, waits for them, and re-layouts: 11.6 us -> 6.71 us
  Pallas kernels: 146 us -> 149 us
  other arithmetic: 5.26 us -> 3.41 us
    unnamed x15 -> x9, local copies, waits for them, and re-layouts: 7.27 us -> 3.79 us
    pallas_call x1, Pallas kernels: 73 us -> 75.7 us  [per_device(): pl.pallas_call(functools.partial(scatter_kernel, (n_rep, n_fs, n_tp, n_y)...]
    concatenate x1 -> x0, other arithmetic: 1.84 us -> none  [per_device(): jnp.concatenate([gate_weight.T.reshape(n_fs, units, depth), up_weight.T.r...]
    transpose x1 -> x0, local copies, waits for them, and re-layouts: 1.77 us -> none  [per_device(): dw = dw.transpose(1, 0, 2, 3).reshape(n_fs, rows, depth)]
where the time goes in v3:
time: 170 us
  Pallas kernels  149 us (88%)
  matrix products  10 us (6%)
  local copies, waits for them, and re-layouts  6.71 us (4%)
  other arithmetic  3.41 us (2%)
    pallas_call x1, Pallas kernels, per_device(): pl.pallas_call(functools.partial(scatter_kernel, (n_rep, n_fs, n_tp, n_y)...  75.7 us
    pallas_call x1, Pallas kernels, per_device(): pl.pallas_call(functools.partial(gather_kernel, (n_rep, n_fs, n_tp, n_y))...  73 us
    dot_general x1, matrix products, per_device(): pre = lax.dot_general(x_all, w_in, last, preferred_element_type=f32)  4.46 us
    unnamed x9, local copies, waits for them, and re-layouts  3.79 us

profile of v3, /device:TPU:0, one launch (start us, length us, event | category | flops | bytes accessed | tf_op | source)
XLA Modules:
  0.0 169.6 jit_solution(1435340646815746221)
XLA Ops:
  0.6 0.1 pad.2.clone
  0.7 73.0 %shard_map.84 = (bf16[8,128,2048]{2,1,0:T(8,128)(2,1)}, bf16[8,128,2048]{2,1,0:T(8,128)(2,1)}, bf16[2,272,2048]{2,1,0:T(8,128)(2,1)}) custom-call(bf16[128,1024]{1,0:T(8,128)(2,1)} %x_ref.1, bf16[128,1024]{1,0:T(8,128)(2,1)} %c_ref.1, bf16[256,1408]{1,0:T(8,128)(2,1)} %refs_0_.1, bf16[256,1408]{1,0:T(8,128)(2,1)} %refs_1_.1, bf16[1408,256]{1,0:T(8,128)(2,1)} %refs_2_.1), custom_call_target="tpu_custom_call" | custom-call | tf_op jit(solution)/shard_map/pallas_call | solution.py:356
  73.7 0.0 copy-start.2
  73.7 4.5 %fusion = f32[1024,352]{0,1:T(8,128)S(1)} fusion(bf16[1024,2048]{1,0:T(8,128)(2,1)} %bitcast.29, bf16[544,2048]{1,0:T(8,128)(2,1)} %bitcast.25), kind=kOutput, calls=%fused_computation.3 | convolution fusion | flops 1476395008 | bytes 7077888 | tf_op jit(solution)/shard_map/dot_general | solution.py:376
  78.2 0.0 copy-done.2
  78.2 0.9 convolution_convert_fusion.1
  79.1 0.0 copy-start.1
  79.2 3.0 %multiply_convert_fusion.2 = (bf16[1024,176]{0,1:T(8,128)(2,1)S(1)}, bf16[1024,176]{0,1:T(8,128)(2,1)S(1)}) fusion(f32[1024,352]{0,1:T(8,128)S(1)} %fusion, bf16[1024,2048]{1,0:T(8,128)(2,1)S(1)} %bitcast.32, bf16[544,2048]{1,0:T(8,128)(2,1)} %bitcast.26), kind=kOutput, calls=%fused_computation.13 | convolution fusion | flops 740540416 | bytes 7077888 | tf_op jit(solution)/shard_map/dot_general | solution.py:377
  82.1 0.0 copy-done.1
  82.1 1.7 convolution_convert_fusion
  83.8 1.8 %maximum_maximum_fusion = bf16[544,2048]{1,0:T(8,128)(2,1)} fusion(bf16[176,2048]{1,0:T(8,128)(2,1)S(1)} %convolution_convert_fusion.1, bf16[352,2048]{1,0:T(8,128)(2,1)S(1)} %convolution_convert_fusion, bf16[544]{0:T(1024)(128)(2,1)S(1)} %pad.2.clone), kind=kLoop, calls=%fused_computation.2 | loop fusion | flops 6684672 | bytes 4392000 | tf_op jit(solution)/shard_map/concatenate | solution.py:387
  85.6 1.2 copy.12
  86.8 75.7 %shard_map.85 = (bf16[128,1024]{1,0:T(8,128)(2,1)}, bf16[8,2,272,256]{3,2,1,0:T(8,128)(2,1)}) custom-call(bf16[8,128,352]{2,1,0:T(8,128)(2,1)} %bitcast.24, bf16[544,2048]{1,0:T(8,128)(2,1)} %bitcast.27, bf16[2,272,2048]{2,1,0:T(8,128)(2,1)} %bitcast.23), custom_call_target="tpu_custom_call" | custom-call | tf_op jit(solution)/shard_map/pallas_call | solution.py:399
  162.5 1.7 fusion.7
  164.2 1.3 bitcast_convert_fusion
  165.5 0.3 convert_bitcast_fusion
  165.8 0.0 copy-start
  165.8 1.5 copy.14
  167.3 1.5 copy.13
  168.9 0.0 copy-done
  168.9 0.7 copy.16
  (2 shorter events, 0.1 us)
Async XLA Ops:
  73.7 4.5 %copy-start.2 = (bf16[8,128,2048]{2,1,0:T(8,128)(2,1)S(1)}, bf16[8,128,2048]{2,1,0:T(8,128)(2,1)}, u32[]{:S(2)}) copy-start(bf16[8,128,2048]{2,1,0:T(8,128)(2,1)} %get-tuple-element.9) | copy-start | bytes 12582916
  79.1 3.0 %copy-start.1 = (bf16[8,128,2048]{2,1,0:T(8,128)(2,1)S(1)}, bf16[8,128,2048]{2,1,0:T(8,128)(2,1)}, u32[]{:S(2)}) copy-start(bf16[8,128,2048]{2,1,0:T(8,128)(2,1)} %get-tuple-element.11) | copy-start | bytes 12582916
  165.8 3.1 %copy-start = (bf16[128,1024]{1,0:T(8,128)(2,1)S(1)}, bf16[128,1024]{1,0:T(8,128)(2,1)}, u32[]{:S(2)}) copy-start(bf16[128,1024]{1,0:T(8,128)(2,1)} %get-tuple-element.29) | copy-start | bytes 786436

commit v4 on v3

--- a/solution.py
+++ b/solution.py
@@ -138,17 +138,26 @@
         w_ref = weights[0]
     else:
         split_weights(weights, w_ref)
-    for k in near_first(n_fs):
-        peer = lax.rem(fs + k, n_fs)
-        out.send(w_ref.at[peer, rep], w_slot(rep, fs), w_recv.at[rep, fs], "fs", peer)
+    offsets = near_first(n_fs)
+    soon, late = offsets[: len(offsets) // 2], offsets[len(offsets) // 2 :]
+    if n_z < 3:
+        soon, late = [], offsets
+
+    def send_weights(group):
+        for k in group:
+            peer = lax.rem(fs + k, n_fs)
+            out.send(w_ref.at[peer, rep], w_slot(rep, fs), w_recv.at[rep, fs], "fs", peer)
+
+    if n_z < 3:
+        send_weights(late)
     for k in range(1, n_rep):
         out.send(
             w_ref.at[fs, rep], w_slot(rep, fs), w_recv.at[rep, fs], "rep", lax.rem(rep + k, n_rep)
         )
     out.local(w_ref.at[fs, rep], w_slot(rep, fs))
 
-    def swap_weights():
-        for k in near_first(n_fs):
+    def swap_weights(group):
+        for k in group:
             owner = lax.rem(fs + n_fs - k, n_fs)
             slot = w_slot(rep, owner)
             arrived(slot, w_recv.at[rep, owner])
@@ -157,8 +166,8 @@
                 out.send(slot, slot, w_recv.at[rep, owner], "rep", peer)
 
     for k in range(1, n_z):
-        if k == max(n_z - 1, 1):
-            swap_weights()
+        if k == n_z - 1:
+            swap_weights(soon)
         for a in range(2):
             for here, onward, step in (
                 (z >= k, z + 1 < n_z, -1), (z + k < n_z, z >= 1, 1)
@@ -172,8 +181,11 @@
                     )
                 to_y(a, owner, slot, here)
                 to_tp(a, owner, slot, here)
-    if n_z == 1:
-        swap_weights()
+        if n_z >= 3 and k == 1:
+            send_weights(soon)
+        if n_z >= 3 and k == n_z - 2:
+            send_weights(late)
+    swap_weights(late)
     for kz in [0] + near_first(n_z):
         for ky in range(1, n_y):
             owner = lax.rem(z + n_z - kz, n_z) * n_y + lax.rem(y + ky, n_y)

time: 170 us -> 169 us (level)
    pallas_call x1, Pallas kernels: 75.7 us -> 72.9 us  [per_device(): pl.pallas_call(functools.partial(scatter_kernel, (n_rep, n_fs, n_tp, n_y)...]
    pallas_call x1, Pallas kernels: 73 us -> 75.3 us  [per_device(): pl.pallas_call(functools.partial(gather_kernel, (n_rep, n_fs, n_tp, n_y))...]
where the time goes in v4:
time: 169 us
  Pallas kernels  148 us (88%)
  matrix products  10 us (6%)
  local copies, waits for them, and re-layouts  6.71 us (4%)
  other arithmetic  3.41 us (2%)
    pallas_call x1, Pallas kernels, per_device(): pl.pallas_call(functools.partial(gather_kernel, (n_rep, n_fs, n_tp, n_y))...  75.3 us
    pallas_call x1, Pallas kernels, per_device(): pl.pallas_call(functools.partial(scatter_kernel, (n_rep, n_fs, n_tp, n_y)...  72.9 us
    dot_general x1, matrix products, per_device(): pre = lax.dot_general(x_all, w_in, last, preferred_element_type=f32)  4.46 us
    unnamed x9, local copies, waits for them, and re-layouts  3.79 us

profile of v4, /device:TPU:0, one launch (start us, length us, event | category | flops | bytes accessed | tf_op | source)
XLA Modules:
  0.0 169.0 jit_solution(2454043383256927473)
XLA Ops:
  0.6 0.1 pad.2.clone
  0.7 75.3 %shard_map.84 = (bf16[8,128,2048]{2,1,0:T(8,128)(2,1)}, bf16[8,128,2048]{2,1,0:T(8,128)(2,1)}, bf16[2,272,2048]{2,1,0:T(8,128)(2,1)}) custom-call(bf16[128,1024]{1,0:T(8,128)(2,1)} %x_ref.1, bf16[128,1024]{1,0:T(8,128)(2,1)} %c_ref.1, bf16[256,1408]{1,0:T(8,128)(2,1)} %refs_0_.1, bf16[256,1408]{1,0:T(8,128)(2,1)} %refs_1_.1, bf16[1408,256]{1,0:T(8,128)(2,1)} %refs_2_.1), custom_call_target="tpu_custom_call" | custom-call | tf_op jit(solution)/shard_map/pallas_call | solution.py:368
  76.0 0.0 copy-start.2
  76.0 4.5 %fusion = f32[1024,352]{0,1:T(8,128)S(1)} fusion(bf16[1024,2048]{1,0:T(8,128)(2,1)} %bitcast.29, bf16[544,2048]{1,0:T(8,128)(2,1)} %bitcast.25), kind=kOutput, calls=%fused_computation.3 | convolution fusion | flops 1476395008 | bytes 7077888 | tf_op jit(solution)/shard_map/dot_general | solution.py:388
  80.5 0.0 copy-done.2
  80.5 0.9 convolution_convert_fusion.1
  81.4 0.0 copy-start.1
  81.4 3.0 %multiply_convert_fusion.2 = (bf16[1024,176]{0,1:T(8,128)(2,1)S(1)}, bf16[1024,176]{0,1:T(8,128)(2,1)S(1)}) fusion(f32[1024,352]{0,1:T(8,128)S(1)} %fusion, bf16[1024,2048]{1,0:T(8,128)(2,1)S(1)} %bitcast.32, bf16[544,2048]{1,0:T(8,128)(2,1)} %bitcast.26), kind=kOutput, calls=%fused_computation.13 | convolution fusion | flops 740540416 | bytes 7077888 | tf_op jit(solution)/shard_map/dot_general | solution.py:389
  84.4 0.0 copy-done.1
  84.4 1.7 convolution_convert_fusion
  86.1 1.8 %maximum_maximum_fusion = bf16[544,2048]{1,0:T(8,128)(2,1)} fusion(bf16[176,2048]{1,0:T(8,128)(2,1)S(1)} %convolution_convert_fusion.1, bf16[352,2048]{1,0:T(8,128)(2,1)S(1)} %convolution_convert_fusion, bf16[544]{0:T(1024)(128)(2,1)S(1)} %pad.2.clone), kind=kLoop, calls=%fused_computation.2 | loop fusion | flops 6684672 | bytes 4392000 | tf_op jit(solution)/shard_map/concatenate | solution.py:399
  87.9 1.2 copy.12
  89.1 72.9 %shard_map.85 = (bf16[128,1024]{1,0:T(8,128)(2,1)}, bf16[8,2,272,256]{3,2,1,0:T(8,128)(2,1)}) custom-call(bf16[8,128,352]{2,1,0:T(8,128)(2,1)} %bitcast.24, bf16[544,2048]{1,0:T(8,128)(2,1)} %bitcast.27, bf16[2,272,2048]{2,1,0:T(8,128)(2,1)} %bitcast.23), custom_call_target="tpu_custom_call" | custom-call | tf_op jit(solution)/shard_map/pallas_call | solution.py:411
  162.0 1.7 %fusion.7 = (bf16[8,176,256]{2,1,0:T(8,128)(2,1)S(1)}, bf16[8,176,256]{2,1,0:T(8,128)(2,1)S(1)}, bf16[8,176,256]{2,1,0:T(8,128)(2,1)S(1)}) fusion(bf16[8,544,256]{2,1,0:T(8,128)(2,1)} %bitcast.28), kind=kLoop, calls=%fused_computation.17 | loop fusion | bytes 4325376 | tf_op jit(solution)/shard_map/slice | solution.py:441
  163.7 1.3 bitcast_convert_fusion
  164.9 0.3 convert_bitcast_fusion
  165.2 0.0 copy-start
  165.3 1.5 copy.14
  166.8 1.5 copy.13
  168.3 0.0 copy-done
  168.3 0.7 copy.16
  (2 shorter events, 0.1 us)
Async XLA Ops:
  76.0 4.5 %copy-start.2 = (bf16[8,128,2048]{2,1,0:T(8,128)(2,1)S(1)}, bf16[8,128,2048]{2,1,0:T(8,128)(2,1)}, u32[]{:S(2)}) copy-start(bf16[8,128,2048]{2,1,0:T(8,128)(2,1)} %get-tuple-element.9) | copy-start | bytes 12582916
  81.4 3.0 %copy-start.1 = (bf16[8,128,2048]{2,1,0:T(8,128)(2,1)S(1)}, bf16[8,128,2048]{2,1,0:T(8,128)(2,1)}, u32[]{:S(2)}) copy-start(bf16[8,128,2048]{2,1,0:T(8,128)(2,1)} %get-tuple-element.11) | copy-start | bytes 12582916
  165.2 3.1 %copy-start = (bf16[128,1024]{1,0:T(8,128)(2,1)S(1)}, bf16[128,1024]{1,0:T(8,128)(2,1)}, u32[]{:S(2)}) copy-start(bf16[128,1024]{1,0:T(8,128)(2,1)} %get-tuple-element.29) | copy-start | bytes 786436
